TPU v7x, 32 devices: a whole 2x2x4 slice. The times are simulated.
32 devices in a mesh: ep: 16 (over z, y, x), tp: 2 (over core).
Axes of the slice: x: 2, y: 2, z: 4, core: 2. Of those that a mesh axis runs over, the one named last changes fastest.
Arguments:
- resid: bfloat16 [256, 2048], P('ep'), may hold values from -6 to 6
- proj_x: bfloat16 [256, 2048], P('ep', 'tp'), may hold values from -6 to 6
- proj_z: bfloat16 [256, 2048], P('ep', 'tp'), may hold values from -6 to 6
- proj_bc: bfloat16 [256, 2, 512], P('ep', None, 'tp'), may hold values from -6 to 6
- proj_dt: bfloat16 [256, 32], P('ep', 'tp'), may hold values from -6 to 6
- tail_x: bfloat16 [256, 3, 2048], P('ep', None, 'tp'), may hold values from -6 to 6
- tail_bc: bfloat16 [256, 3, 2, 512], P('ep', None, None, 'tp'), may hold values from -6 to 6
- taps_x: bfloat16 [4, 2048], P(None, 'tp'), may hold values from -3 to 3
- taps_bc: bfloat16 [4, 2, 512], P(None, None, 'tp'), may hold values from -3 to 3
- ssm_state: float32 [256, 32, 4096], P('ep', 'tp'), may hold values from -1.5 to 1.5
- dt_bias: float32 [32], P('tp'), may hold values from -4 to 0
- decay_log: float32 [32], P('tp'), may hold values from -1 to 2.5
- group_gain: float32 [2048], P('tp'), may hold values from 0.1 to 1.9
- out_proj: bfloat16 [2048, 2048], P('tp', 'ep'), may hold values from -0.125 to 0.125
- ffn_gain: float32 [2048], replicated, may hold values from 0.1 to 1.9
- dense_gate: bfloat16 [2048, 4096], P(None, ('ep', 'tp')), may hold values from -0.125 to 0.125
- dense_up: bfloat16 [2048, 4096], P(None, ('ep', 'tp')), may hold values from -0.125 to 0.125
- dense_down: bfloat16 [4096, 2048], P(('ep', 'tp')), may hold values from -0.09375 to 0.09375
- branch_gate: bfloat16 [2048], replicated, may hold values from -0.125 to 0.125
- group_weights: float32 [256, 4], replicated, may hold values from 0.2 to 1
- expert_ids: int32 [256, 6], replicated, may hold values from 0 to 15, all different within a row; in each aligned block of 16 rows (0 to 15, 16 to 31, ...) at most 7 rows name the same one
- expert_weights: float32 [256, 6], replicated, may hold values from 0.1 to 1
- exp_gate: bfloat16 [16, 2048, 512], P('ep', None, 'tp'), may hold values from -0.125 to 0.125
- exp_up: bfloat16 [16, 2048, 512], P('ep', None, 'tp'), may hold values from -0.125 to 0.125
- exp_down: bfloat16 [16, 512, 2048], P('ep', 'tp'), may hold values from -0.25 to 0.25
Outputs:
- out: bfloat16 [256, 2048], P(('ep', 'tp'))
- new_state: float32 [256, 32, 4096], P('ep', 'tp')
Inputs may be any that keep to these rules, and one draw needn't show every extreme that they name: `expert_ids`: each row names 6 different experts. In the rows of one index of ep (aligned blocks of 16 rows) no expert is named more than 7 times, a bound that some block reaches.
All inputs are finite; a program needn't handle non-finite values.
Results may differ from a plain program's by a relative error of at most 0.013.
Values may be sent and summed in bfloat16 or wider, within the bound.
No kernel may reach another device: no remote copies, remote signals or barrier semaphores. Data moves between devices by JAX's collectives and lax.ppermute only.
A program may use at most 128 MiB of HBM per device.

v0:
```python
import jax
import jax.numpy as jnp
from jax import lax
from jax.sharding import PartitionSpec as P

HEAD_P = 64
NSTATE = 64
GROUPS = 4
TOPK = 6
HPG = 4


EPSILON = 1e-06


def state_update(
    proj_x,
    proj_z,
    proj_bc,
    proj_dt,
    tail_x,
    tail_bc,
    taps_x,
    taps_bc,
    ssm_state,
    dt_bias,
    decay_log,
    group_gain,
):
    window_x = jnp.concatenate([tail_x, proj_x[:, None]], axis=1).astype(jnp.float32)
    conv_x = jax.nn.silu(jnp.sum(window_x * taps_x.astype(jnp.float32)[None], axis=1))
    window_bc = jnp.concatenate([tail_bc, proj_bc[:, None]], axis=1).astype(jnp.float32)
    conv_bc = jax.nn.silu(jnp.sum(window_bc * taps_bc.astype(jnp.float32)[None], axis=1))
    count = proj_x.shape[0]
    heads = proj_dt.shape[1]
    x_heads = conv_x.reshape(count, heads, HEAD_P)
    grouped_bc = conv_bc.reshape(count, 2, heads // HPG, NSTATE)
    input_heads = jnp.repeat(grouped_bc[:, 0], HPG, axis=1)
    read_heads = jnp.repeat(grouped_bc[:, 1], HPG, axis=1)
    step_size = jax.nn.softplus(proj_dt.astype(jnp.float32) + dt_bias)
    decay = jnp.exp(-step_size * jnp.exp(decay_log))
    state = ssm_state.reshape(count, heads, HEAD_P, NSTATE)
    fresh = (step_size[:, :, None] * x_heads)[:, :, :, None] * input_heads[:, :, None, :]
    new_state = decay[:, :, None, None] * state + fresh
    readout = jnp.sum(new_state * read_heads[:, :, None, :], axis=-1)
    gated = readout.reshape(count, heads * HEAD_P) * jax.nn.silu(proj_z.astype(jnp.float32))
    grouped = gated.reshape(count, heads // HPG, HPG * HEAD_P)
    grouped = grouped * lax.rsqrt(jnp.mean(grouped * grouped, axis=-1, keepdims=True) + EPSILON)
    y_out = (grouped.reshape(count, heads * HEAD_P) * group_gain).astype(jnp.bfloat16)
    return (y_out, new_state.reshape(count, heads, HEAD_P * NSTATE))


def shards(
    resid,
    proj_x,
    proj_z,
    proj_bc,
    proj_dt,
    tail_x,
    tail_bc,
    taps_x,
    taps_bc,
    ssm_state,
    dt_bias,
    decay_log,
    group_gain,
    out_proj,
    ffn_gain,
    dense_gate,
    dense_up,
    dense_down,
    branch_gate,
    group_weights,
    expert_ids,
    expert_weights,
    exp_gate,
    exp_up,
    exp_down,
):
    y_out, new_state = state_update(
        proj_x,
        proj_z,
        proj_bc,
        proj_dt,
        tail_x,
        tail_bc,
        taps_x,
        taps_bc,
        ssm_state,
        dt_bias,
        decay_log,
        group_gain,
    )
    partial_value = jnp.dot(
        lax.all_gather(y_out, "ep", axis=0, tiled=True),
        out_proj,
        preferred_element_type=jnp.float32,
    )
    partial_value = lax.all_to_all(
        partial_value.astype(jnp.bfloat16), "ep", split_axis=0, concat_axis=1, tiled=True
    ).astype(partial_value.dtype)
    mixed = lax.psum(partial_value.astype(jnp.bfloat16), "tp").astype(jnp.float32)
    resid_new = (resid.astype(jnp.float32) + mixed).astype(jnp.bfloat16)
    widened = resid_new.astype(jnp.float32)
    normed = (
        widened
        * lax.rsqrt(jnp.mean(widened * widened, axis=-1, keepdims=True) + EPSILON)
        * ffn_gain
    ).astype(jnp.bfloat16)
    gathered = lax.all_gather(normed, "ep", axis=0, tiled=True)
    score = jnp.dot(gathered, branch_gate, preferred_element_type=jnp.float32)
    dense_pre = jnp.dot(gathered, dense_gate, preferred_element_type=jnp.float32)
    dense_lin = jnp.dot(gathered, dense_up, preferred_element_type=jnp.float32)
    dense_hidden = (jax.nn.sigmoid(score)[:, None] * jax.nn.silu(dense_pre) * dense_lin).astype(
        jnp.bfloat16
    )
    experts = lax.axis_size("ep")
    expert_own = lax.axis_index("ep")
    cores = lax.axis_size("tp")
    core_index = lax.axis_index("tp")
    batch = gathered.shape[0]
    rows_each = batch // experts
    half_rows = rows_each // cores
    pairs = rows_each * TOPK
    capacity = (pairs + experts - 1) // experts + 1
    group_size = experts // GROUPS
    levels = jnp.arange(1, capacity + 1, dtype=jnp.int32)
    pair_row = jnp.arange(pairs, dtype=jnp.int32) // TOPK
    pick = (jnp.arange(GROUPS, dtype=jnp.int32) == expert_own // group_size).astype(jnp.float32)
    coarse = jnp.sum(group_weights * pick[None], axis=1)
    pair_weight = (expert_weights * coarse[:, None]).reshape(experts, pairs)
    hits = (expert_ids.reshape(experts, pairs) == expert_own).astype(jnp.int32)
    ranks = jnp.cumsum(hits, axis=1, dtype=jnp.int32)
    select = hits[:, None, :] * (ranks[:, None, :] == levels[None, :, None]).astype(jnp.int32)
    local_row = jnp.sum(select * pair_row[None, None, :], axis=-1, dtype=jnp.int32)
    filled = jnp.sum(select, axis=-1, dtype=jnp.int32).reshape(-1)
    slot_weight = jnp.sum(select.astype(jnp.float32) * pair_weight[:, None, :], axis=-1).reshape(-1)
    row_index = (local_row + jnp.arange(experts, dtype=jnp.int32)[:, None] * rows_each).reshape(-1)
    slot_rows = jnp.take(gathered, row_index, axis=0)
    slot_pre = jnp.dot(slot_rows, exp_gate[0], preferred_element_type=jnp.float32)
    slot_lin = jnp.dot(slot_rows, exp_up[0], preferred_element_type=jnp.float32)
    slot_hidden = (slot_weight[:, None] * jax.nn.silu(slot_pre) * slot_lin).astype(jnp.bfloat16)
    placing = (jnp.arange(batch, dtype=jnp.int32)[:, None] == row_index[None, :]) & (
        filled[None, :] > 0
    )
    row_hidden = jnp.dot(
        placing.astype(jnp.bfloat16), slot_hidden, preferred_element_type=jnp.float32
    ).astype(jnp.bfloat16)
    joined = jnp.concatenate([dense_hidden, row_hidden], axis=1)
    down_all = jnp.concatenate([dense_down, exp_down[0]], axis=0)
    inner_width = joined.shape[1]
    ordered = (
        joined.reshape(experts, cores, half_rows, inner_width)
        .transpose(1, 0, 2, 3)
        .reshape(batch, inner_width)
    )
    halved = lax.psum_scatter(
        jnp.dot(ordered, down_all, preferred_element_type=jnp.float32).astype(jnp.bfloat16),
        "tp",
        scatter_dimension=0,
        tiled=True,
    ).astype(jnp.float32)
    branch = lax.psum_scatter(halved, "ep", scatter_dimension=0, tiled=True)
    own_rows = lax.dynamic_slice_in_dim(widened, core_index * half_rows, half_rows, 0)
    out = (own_rows + branch).astype(jnp.bfloat16)
    return (out, new_state)


def solution(mesh):
    return jax.shard_map(
        shards,
        mesh=mesh,
        in_specs=(
            P("ep", None),
            P("ep", "tp"),
            P("ep", "tp"),
            P("ep", None, "tp"),
            P("ep", "tp"),
            P("ep", None, "tp"),
            P("ep", None, None, "tp"),
            P(None, "tp"),
            P(None, None, "tp"),
            P("ep", "tp", None),
            P("tp"),
            P("tp"),
            P("tp"),
            P("tp", "ep"),
            P(),
            P(None, ("ep", "tp")),
            P(None, ("ep", "tp")),
            P(("ep", "tp"), None),
            P(),
            P(),
            P(),
            P(),
            P("ep", None, "tp"),
            P("ep", None, "tp"),
            P("ep", "tp", None),
        ),
        out_specs=(P(("ep", "tp"), None), P("ep", "tp", None)),
        check_vma=False,
    )
```

profile of v0, /device:TPU:0, one launch (start us, length us, event | category | flops | bytes accessed | tf_op | source)
XLA Modules:
  0.0 270.5 jit_solution(9776574114942145212)
XLA Ops:
  7.2 0.7 exp.39
  8.6 0.9 multiply_reduce_fusion.3
  10.4 0.9 multiply_reduce_fusion.1
  11.5 7.9 %reshape.179 = f32[16,16,64,64]{3,2,1,0:T(8,128)} reshape(f32[16,16,4096]{2,1,0:T(8,128)} %param.34) | data formatting | bytes 8388608 | tf_op jit(solution)/shard_map/reshape | solution.py:42
  19.7 8.5 %broadcast_multiply_fusion = (f32[16,16,64,64]{3,2,1,0:T(8,128)}, f32[16,16,64]{2,1,0:T(8,128)S(1)}) fusion(f32[16,16,64]{2,1,0:T(8,128)S(1)} %bitcast.44, f32[16,16,64]{2,1,0:T(8,128)S(1)} %multiply_multiply_fusion, f32[16,16,64]{2,1,0:T(8,128)S(1)} %bitcast.45, f32[16,16,64,64]{3,2,1,0:T(8,128)} %reshape.179, f32[16,16]{1,0:T(8,128)S(1)} %get-tuple-element.11), kind=kLoop, calls=%fused_computation.3 | loop fusion | flops 5226496 | bytes 8651776 | tf_op jit(solution)/shard_map/mul | solution.py:43
  28.7 45.3 %all_gather.6 = bf16[256,1024]{1,0:T(8,128)(2,1)S(1)} all-gather(bf16[16,1024]{1,0:T(8,128)(2,1)S(1)} %multiply_convert_fusion.1), channel_id=1, replica_groups=mesh['ep'=16,'tp'=2] {'ep'}, dimensions={0}, use_global_device_ids=true | all-gather | bytes 557056 | tf_op jit(solution)/shard_map/all_gather | solution.py:95
  74.0 0.9 convolution_convert_fusion.2
  74.9 3.5 %all-to-all-start = ((bf16[16,16,128]{2,1,0:T(8,128)(2,1)}), bf16[16,16,128]{2,1,0:T(8,128)(2,1)S(1)}, u32[]{:S(2)}, u32[]{:S(2)}) async-start(bf16[16,16,128]{2,1,0:T(8,128)(2,1)} %bitcast.6), calls=%async_computation | async-start | bytes 131072 | tf_op jit(solution)/shard_map/all_to_all | solution.py:99
  78.5 7.4 %all-to-all-done = bf16[16,16,128]{2,1,0:T(8,128)(2,1)S(1)} async-done(((bf16[16,16,128]{2,1,0:T(8,128)(2,1)}), bf16[16,16,128]{2,1,0:T(8,128)(2,1)S(1)}, u32[]{:S(2)}, u32[]{:S(2)}) %all-to-all-start) | async-done | bytes 65568 | tf_op jit(solution)/shard_map/all_to_all | solution.py:99
  86.7 14.5 %all-reduce.2.cloned.1.call-done = bf16[16,2048]{1,0:T(8,128)(2,1)} async-done(((bf16[16,2048]{1,0:T(8,128)(2,1)}), bf16[16,2048]{1,0:T(8,128)(2,1)}) %all-reduce.2.cloned.1.call-update) | async-done | bytes 65552 | tf_op jit(solution)/shard_map/psum | solution.py:102
  101.2 1.0 fusion.21
  102.1 1.6 multiply_convert_fusion
  106.0 54.8 %all-gather.2.cloned.1.call-done = bf16[256,2048]{1,0:T(8,128)(2,1)} async-done(((bf16[16,2048]{1,0:T(8,128)(2,1)}), bf16[256,2048]{1,0:T(8,128)(2,1)}) %all-gather.2.cloned.1.call-update) | async-done | bytes 1048592 | tf_op jit(solution)/shard_map/all_gather | solution.py:110
  160.8 1.6 fusion.36
  162.4 2.8 %gather_fusion = bf16[112,2048]{1,0:T(8,128)(2,1)S(1)} fusion(bf16[256,2048]{1,0:T(8,128)(2,1)} %all-gather.2.cloned.1.call-done, s32[1024]{0:T(1024)S(1)} %pad_clamp_fusion), kind=kCustom, calls=%fused_computation | custom fusion | bytes 917952 | tf_op jit(solution)/shard_map/jit(_take)/gather | solution.py:139
  165.3 1.6 fusion.7
  168.0 1.5 fusion.3
  169.7 3.0 %convolution_convert_fusion = bf16[256,2048]{1,0:T(8,128)(2,1)} fusion(bf16[256,384]{1,0:T(8,128)(2,1)S(1)} %bitcast.48, bf16[256,2048]{1,0:T(8,128)(2,1)} %bitcast.52, bf16[128,2048]{1,0:T(8,128)(2,1)} %param.42), kind=kOutput, calls=%fused_computation.4 | convolution fusion | flops 406323200 | bytes 2818048 | tf_op jit(solution)/shard_map/dot_general | solution.py:158
  172.8 7.3 %reduce-scatter.3.cloned.1.call-done = bf16[128,2048]{1,0:T(8,128)(2,1)} async-done(((bf16[256,2048]{1,0:T(8,128)(2,1)}), bf16[128,2048]{1,0:T(8,128)(2,1)}) %reduce-scatter.3.cloned.1.call-update) | async-done | bytes 524304 | tf_op jit(solution)/shard_map/reduce_scatter | solution.py:157
  180.2 2.2 convert_element_type.106
  182.4 7.9 %mul.284 = f32[16,16,4096]{2,1,0:T(8,128)} reshape(f32[16,16,64,64]{3,2,1,0:T(8,128)} %get-tuple-element.4) | data formatting | bytes 8388608 | tf_op jit(solution)/shard_map/mul | solution.py:43
  190.3 6.6 %multiply_add_fusion = f32[16,16,4096]{2,1,0:T(8,128)} fusion(f32[16,16,4096]{2,1,0:T(8,128)} %mul.284, f32[16,16,4096]{2,1,0:T(8,128)} %param.34, f32[16,16]{1,0:T(8,128)S(1)} %get-tuple-element.11), kind=kLoop, calls=%fused_computation.2 | loop fusion | flops 2097152 | bytes 12583936 | tf_op jit(solution)/shard_map/add | solution.py:44
  196.9 65.7 %reduce-scatter.5.cloned.1.call-done = f32[8,2048]{1,0:T(8,128)} async-done(((f32[128,2048]{1,0:T(8,128)}), f32[8,2048]{1,0:T(8,128)}) %reduce-scatter.5.cloned.1.call-update) | async-done | bytes 65552 | tf_op jit(solution)/shard_map/reduce_scatter | solution.py:163
  262.5 1.5 add_convert_fusion.1
  (89 shorter events, 6.5 us)
Async XLA Ops:
  7.2 159.7 %copy-start = (bf16[1,2048,256]{2,1,0:T(8,128)(2,1)S(1)}, bf16[1,2048,256]{2,1,0:T(8,128)(2,1)}, u32[]{:S(2)}) copy-start(bf16[1,2048,256]{2,1,0:T(8,128)(2,1)} %param.48) | copy-start | bytes 3145732
  11.5 7.9 %copy-start.12 = (bf16[16,16]{1,0:T(8,128)(2,1)S(1)}, bf16[16,16]{1,0:T(8,128)(2,1)}, u32[]{:S(2)}) copy-start(bf16[16,16]{1,0:T(8,128)(2,1)} %param.29) | copy-start | bytes 1540
  11.5 7.9 %copy-start.13 = (f32[16]{0:T(128)S(1)}, f32[16]{0:T(128)}, u32[]{:S(2)}) copy-start(f32[16]{0:T(128)} %param.35) | copy-start | bytes 196
  19.6 8.7 %copy-start.5 = (bf16[16,1024]{1,0:T(8,128)(2,1)S(1)}, bf16[16,1024]{1,0:T(8,128)(2,1)}, u32[]{:S(2)}) copy-start(bf16[16,1024]{1,0:T(8,128)(2,1)} %param.27) | copy-start | bytes 98308
  19.6 9.0 %copy-start.9 = (f32[1024]{0:T(1024)S(1)}, f32[1024]{0:T(1024)}, u32[]{:S(2)}) copy-start(f32[1024]{0:T(1024)} %param.37) | copy-start | bytes 12292
  19.6 54.4 %copy-start.3 = (bf16[1024,128]{1,0:T(8,128)(2,1)S(1)}, bf16[1024,128]{1,0:T(8,128)(2,1)}, u32[]{:S(2)}) copy-start(bf16[1024,128]{1,0:T(8,128)(2,1)} %param.38) | copy-start | bytes 786436
  19.6 67.0 %copy-start.7 = (s32[256,6]{0,1:T(8,128)S(1)}, s32[256,6]{0,1:T(8,128)}, u32[]{:S(2)}) copy-start(s32[256,6]{0,1:T(8,128)} %param.45) | copy-start | bytes 18436
  19.6 81.5 %copy-start.4 = (bf16[16,2048]{1,0:T(8,128)(2,1)S(1)}, bf16[16,2048]{1,0:T(8,128)(2,1)}, u32[]{:S(2)}) copy-start(bf16[16,2048]{1,0:T(8,128)(2,1)} %param.25) | copy-start | bytes 196612
  19.6 82.5 %copy-start.6 = (f32[2048]{0:T(1024)S(1)}, f32[2048]{0:T(1024)}, u32[]{:S(2)}) copy-start(f32[2048]{0:T(1024)} %param.39) | copy-start | bytes 24580
  19.7 85.3 %copy-start.11 = (f32[256,4]{0,1:T(4,128)S(1)}, f32[256,4]{0,1:T(4,128)}, u32[]{:S(2)}) copy-start(f32[256,4]{0,1:T(4,128)} %param.44) | copy-start | bytes 12292
  19.7 85.4 %copy-start.8 = (f32[256,6]{0,1:T(8,128)S(1)}, f32[256,6]{0,1:T(8,128)}, u32[]{:S(2)}) copy-start(f32[256,6]{0,1:T(8,128)} %param.46) | copy-start | bytes 18436
  19.7 86.2 %copy-start.10 = (bf16[2048]{0:T(1024)(128)(2,1)S(1)}, bf16[2048]{0:T(1024)(128)(2,1)}, u32[]{:S(2)}) copy-start(bf16[2048]{0:T(1024)(128)(2,1)} %param.43) | copy-start | bytes 12292
  74.9 11.0 %all-to-all-start = ((bf16[16,16,128]{2,1,0:T(8,128)(2,1)}), bf16[16,16,128]{2,1,0:T(8,128)(2,1)S(1)}, u32[]{:S(2)}, u32[]{:S(2)}) async-start(bf16[16,16,128]{2,1,0:T(8,128)(2,1)} %bitcast.6), calls=%async_computation | async-start | bytes 131072 | tf_op jit(solution)/shard_map/all_to_all | solution.py:99
  78.4 22.7 %all-reduce.2.cloned.1.call-start = ((), (), s32[]{:S(2)}) async-start(), calls=%async_computation.3 | async-start | bytes 131072 | tf_op jit(solution)/shard_map/psum | solution.py:102
  86.6 74.2 %all-gather.2.cloned.1.call-start = ((), (), s32[]{:S(2)}) async-start(), calls=%async_computation.4 | async-start | bytes 1114112 | tf_op jit(solution)/shard_map/all_gather | solution.py:110
  103.7 76.4 %reduce-scatter.3.cloned.1.call-start = ((), (), s32[]{:S(2)}) async-start(), calls=%async_computation.5 | async-start | bytes 1572864 | tf_op jit(solution)/shard_map/reduce_scatter | solution.py:157
  162.4 5.0 %copy-start.1 = (bf16[256,2048]{1,0:T(8,128)(2,1)S(1)}, bf16[256,2048]{1,0:T(8,128)(2,1)}, u32[]{:S(2)}) copy-start(bf16[256,2048]{1,0:T(8,128)(2,1)} %all-gather.2.cloned.1.call-done) | copy-start | bytes 3145732
  162.4 5.1 %copy-start.2 = (bf16[2048,128]{1,0:T(8,128)(2,1)S(1)}, bf16[2048,128]{1,0:T(8,128)(2,1)}, u32[]{:S(2)}) copy-start(bf16[2048,128]{1,0:T(8,128)(2,1)} %param.40) | copy-start | bytes 1572868
  172.8 89.7 %reduce-scatter.5.cloned.1.call-start = ((), (), s32[]{:S(2)}) async-start(), calls=%async_computation.6 | async-start | bytes 1114112 | tf_op jit(solution)/shard_map/reduce_scatter | solution.py:163
Sparse Core Ops, SparseCore 0:
  86.7 14.3 all-reduce.1
  104.5 56.2 all-gather.1
  172.9 7.2 reduce-scatter.2
  182.5 79.9 reduce-scatter.4
where the time goes:
time: 272 us; the launch traced here: 271 us
  waiting for transfers between devices  150 us (55%)
  blocking collectives  45.3 us (17%)
  other arithmetic  25.9 us (10%)
  local copies, waits for them, and re-layouts  21.8 us (8%)
  between operations  14.3 us (5%)
  matrix products  9.75 us (4%)
  starting transfers between devices  3.67 us (1%)
    reduce_scatter x1, waiting for transfers between devices, shards(): branch = lax.psum_scatter(halved, 'ep', scatter_dimension=0, tiled=True)  65.7 us
    all_gather x1, waiting for transfers between devices, shards(): gathered = lax.all_gather(normed, 'ep', axis=0, tiled=True)  54.8 us
    all_gather x1, blocking collectives, shards(): lax.all_gather(y_out, 'ep', axis=0, tiled=True)  45.3 us
    psum x1, waiting for transfers between devices, shards(): lax.psum(partial_value.astype(jnp.bfloat16), 'tp').astype(jnp.float32)  14.5 us
    mul x1, other arithmetic, state_update(): (step_size[:, :, None] * x_heads)[:, :, :, None]  8.51 us
    reshape x1, local copies, waits for them, and re-layouts, state_update(): state = ssm_state.reshape(count, heads, HEAD_P, NSTATE)  7.89 us
    mul x1, local copies, waits for them, and re-layouts, state_update(): (step_size[:, :, None] * x_heads)[:, :, :, None]  7.88 us
    all_to_all x1, waiting for transfers between devices, shards(): lax.all_to_all(partial_value.astype(jnp.bfloat16), 'ep', split_axis=0, co...  7.45 us
  transfers between devices with their start and end apart: 5, of which 5 were waited for; matrix products, arithmetic and copies ran while one was open for 6% of the time, Pallas kernels for 0%

commit v1 on v0

v1 whole, which is shorter than its diff:
```python
import functools

import jax
import jax.numpy as jnp
from jax import lax
from jax.experimental import pallas as pl
from jax.experimental.pallas import tpu as pltpu
from jax.sharding import PartitionSpec as P

HEAD_P = 64
NSTATE = 64
GROUPS = 4
HPG = 4
LANES = 128
STATE_COLS = 512


EPSILON = 1e-06


def split_bf16(value):
    high = value.astype(jnp.bfloat16)
    low = (value - high.astype(jnp.float32)).astype(jnp.bfloat16)
    return high, low


def state_kernel(scaled_ref, decay_ref, input_ref, read_ref, state_ref, new_ref, readout_ref):
    step = pl.program_id(0)
    cols = state_ref.shape[1]
    channels = scaled_ref.shape[1]
    repeats = cols // LANES
    first = step * (cols // NSTATE)
    spread = (
        lax.broadcasted_iota(jnp.int32, (channels, cols), 0)
        == first + lax.broadcasted_iota(jnp.int32, (channels, cols), 1) // NSTATE
    )
    spread = spread.astype(jnp.float32).astype(jnp.bfloat16)
    collect = (
        lax.broadcasted_iota(jnp.int32, (cols, channels), 1)
        == first + lax.broadcasted_iota(jnp.int32, (cols, channels), 0) // NSTATE
    )
    collect = collect.astype(jnp.float32).astype(jnp.bfloat16)
    dot = functools.partial(jnp.dot, preferred_element_type=jnp.float32)
    high, low = split_bf16(scaled_ref[...])
    x_cols = dot(high, spread) + dot(low, spread)
    wide = lambda ref: jnp.concatenate([ref[...]] * repeats, axis=1)
    new = wide(decay_ref) * state_ref[...] + x_cols * wide(input_ref)
    new_ref[...] = new
    high, low = split_bf16(new * wide(read_ref))
    part = dot(high, collect) + dot(low, collect)

    @pl.when(step == 0)
    def _():
        readout_ref[...] = part

    @pl.when(step > 0)
    def _():
        readout_ref[...] += part


def run_state(scaled, decay, inputs, reads, state):
    rows, width = state.shape
    cols = min(STATE_COLS, width)
    whole = lambda shape: pl.BlockSpec(shape, lambda j: (0, 0))
    block = pl.BlockSpec((rows, cols), lambda j: (0, j))
    return pl.pallas_call(
        state_kernel,
        grid=(width // cols,),
        in_specs=[whole(scaled.shape), whole(decay.shape), whole(inputs.shape), whole(reads.shape), block],
        out_specs=[block, whole(scaled.shape)],
        out_shape=[
            jax.ShapeDtypeStruct(state.shape, jnp.float32),
            jax.ShapeDtypeStruct(scaled.shape, jnp.float32),
        ],
    )(scaled, decay, inputs, reads, state)


def state_update(
    proj_x,
    proj_z,
    proj_bc,
    proj_dt,
    tail_x,
    tail_bc,
    taps_x,
    taps_bc,
    ssm_state,
    dt_bias,
    decay_log,
    group_gain,
):
    window_x = jnp.concatenate([tail_x, proj_x[:, None]], axis=1).astype(jnp.float32)
    conv_x = jax.nn.silu(jnp.sum(window_x * taps_x.astype(jnp.float32)[None], axis=1))
    window_bc = jnp.concatenate([tail_bc, proj_bc[:, None]], axis=1).astype(jnp.float32)
    conv_bc = jax.nn.silu(jnp.sum(window_bc * taps_bc.astype(jnp.float32)[None], axis=1))
    count = proj_x.shape[0]
    heads = proj_dt.shape[1]
    x_heads = conv_x.reshape(count, heads, HEAD_P)
    grouped_bc = conv_bc.reshape(count, 2, heads // HPG, NSTATE)
    to_rows = lambda v: jnp.repeat(v, HPG, axis=1).reshape(count * heads, NSTATE)
    twice = lambda v: jnp.concatenate([v] * (LANES // NSTATE), axis=1)
    input_rows = twice(to_rows(grouped_bc[:, 0]))
    read_rows = twice(to_rows(grouped_bc[:, 1]))
    step_size = jax.nn.softplus(proj_dt.astype(jnp.float32) + dt_bias)
    decay = jnp.exp(-step_size * jnp.exp(decay_log))
    decay_rows = jnp.broadcast_to(decay[:, :, None], (count, heads, LANES)).reshape(-1, LANES)
    scaled = (step_size[:, :, None] * x_heads).reshape(count * heads, HEAD_P)
    new_state, readout = run_state(
        scaled, decay_rows, input_rows, read_rows, ssm_state.reshape(count * heads, -1)
    )
    gated = readout.reshape(count, heads * HEAD_P) * jax.nn.silu(proj_z.astype(jnp.float32))
    grouped = gated.reshape(count, heads // HPG, HPG * HEAD_P)
    grouped = grouped * lax.rsqrt(jnp.mean(grouped * grouped, axis=-1, keepdims=True) + EPSILON)
    y_out = (grouped.reshape(count, heads * HEAD_P) * group_gain).astype(jnp.bfloat16)
    return (y_out, new_state.reshape(count, heads, HEAD_P * NSTATE))


def ffn_kernel(
    x_ref, weight_ref, score_ref, dgate_ref, dup_ref, ddown_ref, egate_ref, eup_ref, edown_ref, out_ref
):
    dot = functools.partial(jnp.dot, preferred_element_type=jnp.float32)
    x = x_ref[...]
    scale = jax.nn.sigmoid(dot(x, score_ref[...]))
    dense = (scale * jax.nn.silu(dot(x, dgate_ref[...])) * dot(x, dup_ref[...])).astype(jnp.bfloat16)
    expert = weight_ref[...] * jax.nn.silu(dot(x, egate_ref[...])) * dot(x, eup_ref[...])
    expert = expert.astype(jnp.bfloat16)
    out_ref[...] = (dot(dense, ddown_ref[...]) + dot(expert, edown_ref[...])).astype(jnp.bfloat16)


def run_ffn(x, weight, *weights):
    rows, width = x.shape
    block = min(rows, 256)
    whole = lambda v: pl.BlockSpec(v.shape, lambda i: (0, 0))
    part = lambda cols: pl.BlockSpec((block, cols), lambda i: (i, 0))
    return pl.pallas_call(
        ffn_kernel,
        grid=(rows // block,),
        in_specs=[part(width), part(1)] + [whole(v) for v in weights],
        out_specs=part(width),
        out_shape=jax.ShapeDtypeStruct((rows, width), jnp.bfloat16),
        compiler_params=pltpu.CompilerParams(vmem_limit_bytes=48 * 1024 * 1024),
    )(x, weight, *weights)


def gather_ep(value):
    count = lax.axis_size("ep")
    return lax.all_to_all(
        jnp.broadcast_to(value[None], (count,) + value.shape), "ep", 0, 0, tiled=True
    )


def swap_cores(value):
    return lax.ppermute(value, "tp", [(0, 1), (1, 0)])


def shards(
    resid,
    proj_x,
    proj_z,
    proj_bc,
    proj_dt,
    tail_x,
    tail_bc,
    taps_x,
    taps_bc,
    ssm_state,
    dt_bias,
    decay_log,
    group_gain,
    out_proj,
    ffn_gain,
    dense_gate,
    dense_up,
    dense_down,
    branch_gate,
    group_weights,
    expert_ids,
    expert_weights,
    exp_gate,
    exp_up,
    exp_down,
):
    y_out, new_state = state_update(
        proj_x,
        proj_z,
        proj_bc,
        proj_dt,
        tail_x,
        tail_bc,
        taps_x,
        taps_bc,
        ssm_state,
        dt_bias,
        decay_log,
        group_gain,
    )
    experts = lax.axis_size("ep")
    expert_own = lax.axis_index("ep")
    cores = lax.axis_size("tp")
    core = lax.axis_index("tp")
    rows_each, width = resid.shape
    half = rows_each // cores
    partial_value = jnp.dot(
        gather_ep(y_out).reshape(experts * rows_each, -1),
        out_proj,
        preferred_element_type=jnp.float32,
    ).astype(jnp.bfloat16)
    pieces = lax.all_to_all(
        partial_value.reshape(experts * cores, half, -1), ("ep", "tp"), 0, 0, tiled=True
    ).astype(jnp.float32)
    mixed = jnp.sum(pieces.reshape(experts, cores, half, -1), axis=1)
    mixed = mixed.transpose(1, 0, 2).reshape(half, width)
    own = lax.dynamic_slice_in_dim(resid, core * half, half, 0)
    resid_new = (own.astype(jnp.float32) + mixed).astype(jnp.bfloat16)
    widened = resid_new.astype(jnp.float32)
    normed = (
        widened
        * lax.rsqrt(jnp.mean(widened * widened, axis=-1, keepdims=True) + EPSILON)
        * ffn_gain
    ).astype(jnp.bfloat16)
    near = gather_ep(normed).reshape(experts * half, width)
    far = swap_cores(near)
    pick = (jnp.arange(GROUPS, dtype=jnp.int32) == expert_own // (experts // GROUPS)).astype(
        jnp.float32
    )
    coarse = jnp.sum(group_weights * pick[None], axis=1)
    fine = jnp.sum(jnp.where(expert_ids == expert_own, expert_weights, 0.0), axis=1)
    weight = (fine * coarse).reshape(experts, cores, half)
    near_weight = lax.dynamic_index_in_dim(weight, core, 1, keepdims=False).reshape(-1, 1)
    far_weight = lax.dynamic_index_in_dim(weight, 1 - core, 1, keepdims=False).reshape(-1, 1)
    score = jnp.broadcast_to(branch_gate[:, None], (width, dense_gate.shape[1]))
    weights = (score, dense_gate, dense_up, dense_down, exp_gate[0], exp_up[0], exp_down[0])
    near_part = run_ffn(near, near_weight, *weights)
    far_part = run_ffn(far, far_weight, *weights)
    both = near_part.astype(jnp.float32) + swap_cores(far_part).astype(jnp.float32)
    pieces = lax.all_to_all(
        both.astype(jnp.bfloat16).reshape(experts, half, width), "ep", 0, 0, tiled=True
    )
    branch = jnp.sum(pieces.astype(jnp.float32), axis=0)
    return ((widened + branch).astype(jnp.bfloat16), new_state)


def solution(mesh):
    return jax.shard_map(
        shards,
        mesh=mesh,
        in_specs=(
            P("ep", None),
            P("ep", "tp"),
            P("ep", "tp"),
            P("ep", None, "tp"),
            P("ep", "tp"),
            P("ep", None, "tp"),
            P("ep", None, None, "tp"),
            P(None, "tp"),
            P(None, None, "tp"),
            P("ep", "tp", None),
            P("tp"),
            P("tp"),
            P("tp"),
            P("tp", "ep"),
            P(),
            P(None, ("ep", "tp")),
            P(None, ("ep", "tp")),
            P(("ep", "tp"), None),
            P(),
            P(),
            P(),
            P(),
            P("ep", None, "tp"),
            P("ep", None, "tp"),
            P("ep", "tp", None),
        ),
        out_specs=(P(("ep", "tp"), None), P("ep", "tp", None)),
        check_vma=False,
    )
```

time: 272 us -> 107 us (0.39)
  waiting for transfers between devices: 150 us -> 8.25 us
  other arithmetic: 25.9 us -> 8.01 us
  blocking collectives: 45.3 us -> 60.7 us
  Pallas kernels: 0 us -> 14.6 us
  between operations: 14.3 us -> 0.98 us
  local copies, waits for them, and re-layouts: 21.8 us -> 9.94 us
  matrix products: 9.75 us -> 0.92 us
    reduce_scatter x2 -> x0, waiting for transfers between devices: 73 us -> none  [the longest x1 65.7 us: shards(): branch = lax.psum_scatter(halved, 'ep', scatter_dimension=0, tiled=True)]
    all_to_all x0 -> x3, blocking collectives: none -> 60.7 us  [the longest x2 41.3 us: gather_ep(): lax.all_to_all(jnp.broadcast_to(value[None], (count,) + value.shape), 'ep...]
    all_gather x1 -> x0, waiting for transfers between devices: 54.8 us -> none  [shards(): gathered = lax.all_gather(normed, 'ep', axis=0, tiled=True)]
    all_gather x1 -> x0, blocking collectives: 45.3 us -> none  [shards(): lax.all_gather(y_out, 'ep', axis=0, tiled=True)]
    pallas_call x0 -> x3, Pallas kernels: none -> 14.6 us  [the longest x1 8.71 us: run_state(): pl.pallas_call(state_kernel, grid=(width // cols,), in_specs=[whole(scale...]
    psum x1 -> x0, waiting for transfers between devices: 14.5 us -> none  [shards(): lax.psum(partial_value.astype(jnp.bfloat16), 'tp').astype(jnp.float32)]
    dot_general x7 -> x1, matrix products: 9.75 us -> 0.92 us  [shards(): jnp.dot(gather_ep(y_out).reshape(experts * rows_each, -1), out_proj, pref...]
    mul x4 -> x2, local copies, waits for them, and re-layouts: 8.22 us -> 0.18 us  [the longest x1 0.1 us: shards(): weight = (fine * coarse).reshape(experts, cores, half)]
  transfers between devices with their start and end apart: 5 -> 3, of which waited for: 5 -> 2; matrix products, arithmetic and copies ran while one was open for 6% -> 0% of each run, Pallas kernels for 0% -> 2%
where the time goes in v1:
time: 107 us; the launch traced here: 106 us
  blocking collectives  60.7 us (57%)
  Pallas kernels  14.6 us (14%)
  local copies, waits for them, and re-layouts  9.94 us (9%)
  waiting for transfers between devices  8.25 us (8%)
  other arithmetic  8.01 us (7%)
  starting transfers between devices  3.07 us (3%)
    all_to_all x2, blocking collectives, gather_ep(): lax.all_to_all(jnp.broadcast_to(value[None], (count,) + value.shape), 'ep...  41.3 us
    all_to_all x1, blocking collectives, shards(): lax.all_to_all(both.astype(jnp.bfloat16).reshape(experts, half, width), '...  19.3 us
    pallas_call x1, Pallas kernels, run_state(): pl.pallas_call(state_kernel, grid=(width // cols,), in_specs=[whole(scale...  8.71 us
    all_to_all x1, waiting for transfers between devices, shards(): lax.all_to_all(partial_value.reshape(experts * cores, half, -1), ('ep', '...  7.4 us
    unnamed x37, local copies, waits for them, and re-layouts  6.08 us
    pallas_call x2, Pallas kernels, run_ffn(): pl.pallas_call(ffn_kernel, grid=(rows // block,), in_specs=[part(width),...  5.86 us
    all_to_all x1, starting transfers between devices, shards(): lax.all_to_all(partial_value.reshape(experts * cores, half, -1), ('ep', '...  2.93 us
  transfers between devices with their start and end apart: 3, of which 2 were waited for; matrix products, arithmetic and copies ran while one was open for 0% of the time, Pallas kernels for 2%

profile of v1, /device:TPU:0, one launch (start us, length us, event | category | flops | bytes accessed | tf_op | source)
XLA Modules:
  0.0 106.4 jit_solution(7777596861083921147)
XLA Ops:
  2.1 0.7 multiply_exponential_fusion
  3.7 0.9 multiply_reduce_fusion.1
  4.8 0.9 multiply_reduce_fusion
  5.8 0.7 multiply_multiply_fusion.scaled_ref
  6.6 0.8 pad_maximum_fusion
  7.5 0.8 broadcast_in_dim.23.decay_ref
  8.2 8.7 %shard_map.248 = (f32[256,4096]{1,0:T(8,128)}, f32[256,64]{1,0:T(8,128)}) custom-call(f32[256,64]{1,0:T(8,128)} %multiply_multiply_fusion.scaled_ref, f32[256,128]{1,0:T(8,128)} %broadcast_in_dim.23.decay_ref, f32[256,128]{1,0:T(8,128)} %get-tuple-element.14.input_ref, f32[256,128]{1,0:T(8,128)} %get-tuple-element.15.read_ref, f32[256,4096]{1,0:T(8,128)} %bitcast.41), custom_call_target="tpu_custom_call" | custom-call | tf_op jit(solution)/shard_map/pallas_call | solution.py:66
  17.0 1.1 %reshape.94 = f32[16,1024]{1,0:T(8,128)S(1)} reshape(f32[256,64]{1,0:T(8,128)} %get-tuple-element.4) | data formatting | bytes 131072 | tf_op jit(solution)/shard_map/reshape | solution.py:111
  18.5 23.2 %all_to_all.20 = bf16[16,16,1024]{2,1,0:T(8,128)(2,1)S(1)} all-to-all(bf16[16,16,1024]{2,1,0:T(8,128)(2,1)S(1)} %broadcast_in_dim.28), channel_id=1, replica_groups=mesh['ep'=16,'tp'=2] {'ep'}, dimensions={0} | all-to-all | bytes 1048576 | tf_op jit(solution)/shard_map/all_to_all | solution.py:147
  41.8 0.9 fusion
  42.7 2.9 %all-to-all-start.1 = ((bf16[32,8,128]{2,1,0:T(8,128)(2,1)}), bf16[32,8,128]{2,1,0:T(8,128)(2,1)S(1)}, u32[]{:S(2)}, u32[]{:S(2)}) async-start(bf16[32,8,128]{2,1,0:T(8,128)(2,1)} %fusion), calls=%async_computation.1 | async-start | bytes 131072 | tf_op jit(solution)/shard_map/all_to_all | solution.py:208
  45.6 7.4 %all-to-all-done.1 = bf16[32,8,128]{2,1,0:T(8,128)(2,1)S(1)} async-done(((bf16[32,8,128]{2,1,0:T(8,128)(2,1)}), bf16[32,8,128]{2,1,0:T(8,128)(2,1)S(1)}, u32[]{:S(2)}, u32[]{:S(2)}) %all-to-all-start.1) | async-done | bytes 65568 | tf_op jit(solution)/shard_map/all_to_all | solution.py:208
  53.3 18.1 %all_to_all.21 = bf16[16,8,2048]{2,1,0:T(8,128)(2,1)S(1)} all-to-all(bf16[16,8,2048]{2,1,0:T(8,128)(2,1)S(1)} %broadcast_in_dim.29), channel_id=1, replica_groups=mesh['ep'=16,'tp'=2] {'ep'}, dimensions={0} | all-to-all | bytes 1048576 | tf_op jit(solution)/shard_map/all_to_all | solution.py:147
  71.4 0.8 copy-done.8
  72.6 0.8 collective-permute-done.x_ref
  73.9 1.0 copy-done.4
  74.9 1.0 copy-done.6
  75.9 3.4 %shard_map.250 = bf16[128,2048]{1,0:T(8,128)(2,1)} custom-call(bf16[128,2048]{1,0:T(8,128)(2,1)} %collective-permute-done.x_ref, f32[128,1]{1,0:T(8,128)S(1)} %reshape.108.weight_ref, bf16[2048,128]{1,0:T(8,128)(2,1)S(1)} %broadcast_in_dim.31.score_ref, bf16[2048,128]{1,0:T(8,128)(2,1)S(1)} %copy-done.3, bf16[2048,128]{1,0:T(8,128)(2,1)S(1)} %copy-done.4, ...), custom_call_target="tpu_custom_call" | custom-call | tf_op jit(solution)/shard_map/pallas_call | solution.py:135
  79.6 1.0 copy-done.5
  80.6 1.0 copy-done.7
  81.7 1.0 copy-done.9
  82.7 2.5 %shard_map.249 = bf16[128,2048]{1,0:T(8,128)(2,1)S(1)} custom-call(bf16[128,2048]{1,0:T(8,128)(2,1)S(1)} %bitcast.38, f32[128,1]{1,0:T(8,128)S(1)} %reshape.107.weight_ref, bf16[2048,128]{1,0:T(8,128)(2,1)S(1)} %broadcast_in_dim.31.score_ref, bf16[2048,128]{1,0:T(8,128)(2,1)S(1)} %copy-done.3, bf16[2048,128]{1,0:T(8,128)(2,1)S(1)} %copy-done.5, ...), custom_call_target="tpu_custom_call" | custom-call | tf_op jit(solution)/shard_map/pallas_call | solution.py:135
  85.2 1.2 %fusion.1 = bf16[16,8,2048]{2,1,0:T(8,128)(2,1)S(1)} fusion(bf16[128,2048]{1,0:T(8,128)(2,1)} %collective-permute-done.1, bf16[128,2048]{1,0:T(8,128)(2,1)S(1)} %shard_map.249), kind=kLoop, calls=%fused_computation.4 | loop fusion | flops 1048576 | bytes 1572864 | tf_op jit(solution)/shard_map/reshape | solution.py:237
  86.3 19.3 %all_to_all.22 = bf16[16,8,2048]{2,1,0:T(8,128)(2,1)S(1)} all-to-all(bf16[16,8,2048]{2,1,0:T(8,128)(2,1)S(1)} %fusion.1), channel_id=1, replica_groups=mesh['ep'=16,'tp'=2] {'ep'}, dimensions={0} | all-to-all | bytes 1048576 | tf_op jit(solution)/shard_map/all_to_all | solution.py:236
  (68 shorter events, 4.9 us)
Async XLA Ops:
  0.6 41.1 %copy-start = (bf16[1024,128]{1,0:T(8,128)(2,1)S(1)}, bf16[1024,128]{1,0:T(8,128)(2,1)}, u32[]{:S(2)}) copy-start(bf16[1024,128]{1,0:T(8,128)(2,1)} %param.38) | copy-start | bytes 786436
  0.6 17.5 %copy-start.10 = (bf16[16,1024]{1,0:T(8,128)(2,1)S(1)}, bf16[16,1024]{1,0:T(8,128)(2,1)}, u32[]{:S(2)}) copy-start(bf16[16,1024]{1,0:T(8,128)(2,1)} %param.27) | copy-start | bytes 98308
  0.7 17.8 %copy-start.16 = (f32[1024]{0:T(1024)S(1)}, f32[1024]{0:T(1024)}, u32[]{:S(2)}) copy-start(f32[1024]{0:T(1024)} %param.37) | copy-start | bytes 12292
  8.2 44.8 %copy-start.11 = (bf16[16,2048]{1,0:T(8,128)(2,1)S(1)}, bf16[16,2048]{1,0:T(8,128)(2,1)}, u32[]{:S(2)}) copy-start(bf16[16,2048]{1,0:T(8,128)(2,1)} %param.25) | copy-start | bytes 196612
  8.2 45.0 %copy-start.12 = (f32[2048]{0:T(1024)S(1)}, f32[2048]{0:T(1024)}, u32[]{:S(2)}) copy-start(f32[2048]{0:T(1024)} %param.39) | copy-start | bytes 24580
  8.2 64.1 %copy-start.13 = (f32[256,6]{0,1:T(8,128)S(1)}, f32[256,6]{0,1:T(8,128)}, u32[]{:S(2)}) copy-start(f32[256,6]{0,1:T(8,128)} %param.46) | copy-start | bytes 18436
  8.2 64.1 %copy-start.14 = (s32[256,6]{0,1:T(8,128)S(1)}, s32[256,6]{0,1:T(8,128)}, u32[]{:S(2)}) copy-start(s32[256,6]{0,1:T(8,128)} %param.45) | copy-start | bytes 18436
  8.2 64.1 %copy-start.17 = (f32[256,4]{0,1:T(4,128)S(1)}, f32[256,4]{0,1:T(4,128)}, u32[]{:S(2)}) copy-start(f32[256,4]{0,1:T(4,128)} %param.44) | copy-start | bytes 12292
  8.2 65.3 %copy-start.15 = (bf16[2048]{0:T(1024)(128)(2,1)S(1)}, bf16[2048]{0:T(1024)(128)(2,1)}, u32[]{:S(2)}) copy-start(bf16[2048]{0:T(1024)(128)(2,1)} %param.43) | copy-start | bytes 12292
  17.0 56.9 %copy-start.1 = (bf16[1,2048,256]{2,1,0:T(8,128)(2,1)S(1)}, bf16[1,2048,256]{2,1,0:T(8,128)(2,1)}, u32[]{:S(2)}) copy-start(bf16[1,2048,256]{2,1,0:T(8,128)(2,1)} %param.47) | copy-start | bytes 3145732
  17.0 56.9 %copy-start.2 = (bf16[1,2048,256]{2,1,0:T(8,128)(2,1)S(1)}, bf16[1,2048,256]{2,1,0:T(8,128)(2,1)}, u32[]{:S(2)}) copy-start(bf16[1,2048,256]{2,1,0:T(8,128)(2,1)} %param.48) | copy-start | bytes 3145732
  17.0 56.9 %copy-start.3 = (bf16[2048,128]{1,0:T(8,128)(2,1)S(1)}, bf16[2048,128]{1,0:T(8,128)(2,1)}, u32[]{:S(2)}) copy-start(bf16[2048,128]{1,0:T(8,128)(2,1)} %dgate_ref.3) | copy-start | bytes 1572868
  42.7 10.3 %all-to-all-start.1 = ((bf16[32,8,128]{2,1,0:T(8,128)(2,1)}), bf16[32,8,128]{2,1,0:T(8,128)(2,1)S(1)}, u32[]{:S(2)}, u32[]{:S(2)}) async-start(bf16[32,8,128]{2,1,0:T(8,128)(2,1)} %fusion), calls=%async_computation.1 | async-start | bytes 131072 | tf_op jit(solution)/shard_map/all_to_all | solution.py:208
  71.4 2.0 %collective-permute-start = (bf16[128,2048]{1,0:T(8,128)(2,1)S(1)}, bf16[128,2048]{1,0:T(8,128)(2,1)}, u32[]{:S(2)}, u32[]{:S(2)}) collective-permute-start(bf16[128,2048]{1,0:T(8,128)(2,1)S(1)} %bitcast.37), channel_id=1, source_target_pairs={{0,1},{1,0},{2,3},{3,2},{4,5},{5,4},{6,7},{7,6},{8,9},{9,8},{10,11... | collective-permute-start | bytes 1572872 | tf_op jit(solution)/shard_map/ppermute | solution.py:153
  71.4 0.8 copy-start.8
  73.9 1.0 copy-start.4
  74.9 1.0 copy-start.6
  79.4 5.8 %collective-permute-start.1 = (bf16[128,2048]{1,0:T(8,128)(2,1)}, bf16[128,2048]{1,0:T(8,128)(2,1)}, u32[]{:S(2)}, u32[]{:S(2)}) collective-permute-start(bf16[128,2048]{1,0:T(8,128)(2,1)} %shard_map.250), channel_id=1, source_target_pairs={{0,1},{1,0},{2,3},{3,2},{4,5},{5,4},{6,7},{7,6},{8,9},{9,8},{10,11... | collective-permute-start | bytes 1572872 | tf_op jit(solution)/shard_map/ppermute | solution.py:153
  79.6 1.0 copy-start.5
  80.6 1.0 copy-start.7
  81.7 1.0 copy-start.9
